TPU v7x, 128 devices: a whole 4x4x4 slice. The times are simulated.
128 devices in a mesh: fs: 16 (over z, y), tp: 8 (over x, core).
Axes of the slice: x: 4, y: 4, z: 4, core: 2. Of those that a mesh axis runs over, the one named last changes fastest.
Arguments:
- resid: bfloat16 [24576, 2048], P(('fs', 'tp')), may hold values from -6 to 6
- norm1_gain: float32 [2048], replicated, may hold values from 0.1 to 1.9
- w_value: float32 [2048, 2048], P('fs', 'tp'), may hold values from -0.125 to 0.125
- w_gate: float32 [2048, 2048], P('fs', 'tp'), may hold values from -0.125 to 0.125
- value_scale: float32 [2048], replicated, may hold values from 0.3 to 3
- gate_scale: float32 [2048], replicated, may hold values from 0.5 to 3
- conv_taps: float32 [31, 2048], replicated, may hold values from -1 to 1
- conv_gain: float32 [2048], replicated, may hold values from 0.1 to 1.9
- w_point: float32 [2048, 2048], P('tp', 'fs'), may hold values from -0.125 to 0.125
- point_scale: float32 [2048], P('fs'), may hold values from 0.5 to 3
- norm2_gain: float32 [2048], replicated, may hold values from 0.1 to 1.9
- w_up: float32 [2048, 8192], P('fs', 'tp'), may hold values from -0.125 to 0.125
- up_scale: float32 [8192], P('tp'), may hold values from 0.5 to 1.5
- w_down: float32 [8192, 2048], P('tp', 'fs'), may hold values from -0.0625 to 0.0625
- down_scale: float32 [2048], P('fs'), may hold values from 0.3 to 1
Outputs:
- layer_out: bfloat16 [24576, 2048], P(('fs', 'tp'))
All inputs are finite; a program needn't handle non-finite values.
Results may differ from a plain program's by a relative error of at most 0.015.
Values may be sent and summed in bfloat16 or wider, within the bound.
A program may use at most 128 MiB of HBM per device.

v0:
```python
import jax
import jax.numpy as jnp
from jax import lax
from jax.sharding import PartitionSpec as P

GROUPS = 4


def gather_turned(arrays, axis, dims):
    turned = [jnp.moveaxis(a, dim, 0) for a, dim in zip(arrays, dims)]
    both = jnp.concatenate([t.reshape(len(t), -1) for t in turned], axis=1)
    result, at, done = (lax.all_gather(both, axis, axis=0, tiled=True), 0, [])
    for t, dim in zip(turned, dims):
        slab = result[:, at : at + t[0].size].reshape(-1, *t.shape[1:])
        done.append(jnp.moveaxis(slab, 0, dim))
        at += t[0].size
    return tuple(done)


def laid_out(pieces, dim):
    shape = list(pieces.shape[1:])
    shape[dim] *= pieces.shape[0]
    return jnp.moveaxis(pieces, 0, dim).reshape(shape)


def from_everyone(x, axis):
    copies = jnp.broadcast_to(x, (lax.axis_size(axis), *x.shape))
    return lax.all_to_all(copies, axis, split_axis=0, concat_axis=0, tiled=True)


def gather_directly(x, axis, dim):
    return laid_out(from_everyone(x, axis), dim)


def over_copies(x, axis):
    return from_everyone(x, axis).sum(axis=0)


def in_one(arrays, axis):
    ends = [0]
    for a in arrays:
        ends.append(ends[-1] + a.size)
    running = over_copies(jnp.concatenate([a.ravel() for a in arrays]), axis)
    return tuple((running[b:e].reshape(a.shape) for a, b, e in zip(arrays, ends, ends[1:])))


def rms_scaled(values, gain):
    data = values.astype(jnp.float32)
    return data * lax.rsqrt(jnp.mean(data * data, axis=-1, keepdims=True) + 1e-06) * gain


def depthwise(padded, taps, length):
    wide = padded.astype(jnp.float32)
    conv = jnp.zeros((length, wide.shape[1]), jnp.float32)
    for offset in range(taps.shape[0]):
        conv = conv + taps[offset] * wide[offset : offset + length]
    return conv


def fetch_mlp(up_bf, down_bf):
    return gather_turned((up_bf, down_bf), "fs", (0, 1))


def shards(
    resid,
    norm1_gain,
    w_value,
    w_gate,
    value_scale,
    gate_scale,
    conv_taps,
    conv_gain,
    w_point,
    point_scale,
    norm2_gain,
    w_up,
    up_scale,
    w_down,
    down_scale,
):
    tok_rows = resid.shape[0]
    tp_count = lax.axis_size("tp")
    tp_rank = lax.axis_index("tp")
    seq_len = tok_rows * tp_count
    channels = value_scale.shape[0]
    group_width = channels // GROUPS
    reach = conv_taps.shape[0] // 2
    value_bf = w_value.astype(jnp.bfloat16)
    gate_bf = w_gate.astype(jnp.bfloat16)
    point_bf = w_point.astype(jnp.bfloat16)
    up_bf = w_up.astype(jnp.bfloat16)
    down_bf = w_down.astype(jnp.bfloat16)
    point_full, down_full = gather_turned((point_scale, down_scale), "fs", (0, 0))
    normed = rms_scaled(resid, norm1_gain).astype(jnp.bfloat16)
    value_rows, gate_rows, point_rows = gather_turned(
        (value_bf, gate_bf, point_bf), "fs", (0, 0, 1)
    )
    own_width = value_rows.shape[1]
    first = tp_rank * own_width
    own_value_scale = lax.dynamic_slice_in_dim(value_scale, first, own_width, 0)
    own_gate_scale = lax.dynamic_slice_in_dim(gate_scale, first, own_width, 0)
    own_taps = lax.dynamic_slice_in_dim(conv_taps, first, own_width, 1)
    own_gain = lax.dynamic_slice_in_dim(conv_gain, first, own_width, 0)
    piece = gather_directly(normed, "tp", 0)
    value = jnp.dot(piece, value_rows, preferred_element_type=jnp.float32) * own_value_scale
    gate = jnp.dot(piece, gate_rows, preferred_element_type=jnp.float32) * own_gate_scale
    glu_seq = (value * jax.nn.sigmoid(gate)).astype(jnp.bfloat16)
    padded = jnp.pad(glu_seq, ((reach, reach), (0, 0)))
    conv = depthwise(padded, own_taps, seq_len)
    member = ((first + jnp.arange(own_width)) % GROUPS)[:, None] == jnp.arange(GROUPS)[None, :]
    member = member.astype(jnp.float32)
    sums = jnp.dot(conv, member, precision=lax.Precision.HIGHEST)
    squares = jnp.dot(conv * conv, member, precision=lax.Precision.HIGHEST)
    totals, square_totals = in_one((sums, squares), "tp")
    gmean = jnp.dot(totals / group_width, member.T, precision=lax.Precision.HIGHEST)
    gsquare = jnp.dot(square_totals / group_width, member.T, precision=lax.Precision.HIGHEST)
    scaled = (conv - gmean) * lax.rsqrt(gsquare - gmean * gmean + 1e-05) * own_gain
    act = jax.nn.silu(scaled).astype(jnp.bfloat16)
    mixed = lax.psum_scatter(
        jnp.dot(act, point_rows, preferred_element_type=jnp.float32) * point_full,
        "tp",
        scatter_dimension=0,
        tiled=True,
    )
    middle = (resid.astype(jnp.float32) + mixed).astype(jnp.bfloat16)
    normed2 = rms_scaled(middle, norm2_gain).astype(jnp.bfloat16)
    up_cols, down_part = fetch_mlp(up_bf, down_bf)
    upper = (
        jnp.dot(gather_directly(normed2, "tp", 0), up_cols, preferred_element_type=jnp.float32)
        * up_scale
    )
    hidden = jnp.square(jax.nn.relu(upper)).astype(jnp.bfloat16)
    total = lax.psum_scatter(
        (jnp.dot(hidden, down_part, preferred_element_type=jnp.float32) * down_full).astype(
            jnp.bfloat16
        ),
        "tp",
        scatter_dimension=0,
        tiled=True,
    ).astype(jnp.float32)
    return (middle.astype(jnp.float32) + total).astype(jnp.bfloat16)


def solution(mesh):
    in_specs = (
        P(("fs", "tp"), None),
        P(),
        P("fs", "tp"),
        P("fs", "tp"),
        P(),
        P(),
        P(),
        P(),
        P("tp", "fs"),
        P("fs"),
        P(),
        P("fs", "tp"),
        P("tp"),
        P("tp", "fs"),
        P("fs"),
    )
    out_specs = P(("fs", "tp"), None)
    return jax.shard_map(shards, mesh=mesh, in_specs=in_specs, out_specs=out_specs, check_vma=False)
```

profile of v0, /device:TPU:1, one launch (start us, length us, event | category | flops | bytes accessed | tf_op | source)
XLA Modules:
  0.0 365.7 jit_solution(16230646207649153275)
XLA Ops:
  6.5 1.0 convert_bitcast_fusion.1
  7.5 1.0 copy.29
  8.5 1.0 copy.30
  9.6 0.7 pad_maximum_fusion.1
  10.3 0.0 all-gather.3.cloned.1.call-update
  10.3 0.2 fusion.16
  10.6 0.3 fusion.18
  10.8 3.5 broadcast_in_dim.6
  14.3 6.2 %all-to-all-start = ((bf16[8,192,2048]{2,1,0:T(8,128)(2,1)}), bf16[8,192,2048]{2,1,0:T(8,128)(2,1)}, u32[]{:S(2)}, u32[]{:S(2)}) async-start(bf16[8,192,2048]{2,1,0:T(8,128)(2,1)} %broadcast_in_dim.6), calls=%async_computation | async-start | bytes 12582912 | tf_op jit(solution)/shard_map/all_to_all | solution.py:28
  20.4 0.8 dynamic_slice.14
  21.2 0.8 dynamic_slice.13
  22.0 0.8 dynamic_slice.15
  22.7 21.5 %all_gather.10 = f32[2048,2]{0,1:T(2,128)S(1)} all-gather(f32[128,2]{0,1:T(2,128)S(1)} %pad_maximum_fusion.3), channel_id=1, replica_groups=mesh['fs'=16,'tp'=8] {'fs'}, dimensions={0}, use_global_device_ids=true | all-gather | bytes 17408 | tf_op jit(solution)/shard_map/all_gather | solution.py:12
  44.2 1.1 fusion.68
  45.3 1.2 constant_dynamic-slice_fusion
  46.5 45.2 %all-to-all-done = bf16[8,192,2048]{2,1,0:T(8,128)(2,1)} async-done(((bf16[8,192,2048]{2,1,0:T(8,128)(2,1)}), bf16[8,192,2048]{2,1,0:T(8,128)(2,1)}, u32[]{:S(2)}, u32[]{:S(2)}) %all-to-all-start) | async-done | bytes 6291488 | tf_op jit(solution)/shard_map/all_to_all | solution.py:28
  91.7 5.0 %fusion.14 = f32[1536,256]{1,0:T(8,128)S(1)} fusion(bf16[1536,2048]{1,0:T(8,128)(2,1)} %bitcast.1, bf16[2048,768]{0,1:T(8,128)(2,1)} %all-gather.3.cloned.1.call-done, f32[256]{0:T(256)S(1)} %dynamic_slice.14), kind=kOutput, calls=%fused_computation.18 | convolution fusion | flops 1612185600 | bytes 8913920 | tf_op jit(solution)/shard_map/dot_general | solution.py:106
  96.7 4.9 %fusion.15 = bf16[1536,256]{1,0:T(8,128)(2,1)S(1)} fusion(f32[1536,256]{1,0:T(8,128)S(1)} %fusion.14, bf16[1536,2048]{1,0:T(8,128)(2,1)} %bitcast.1, bf16[2048,768]{0,1:T(8,128)(2,1)} %all-gather.3.cloned.1.call-done, f32[256]{0:T(256)S(1)} %dynamic_slice.13), kind=kOutput, calls=%fused_computation.19 | convolution fusion | flops 1611792384 | bytes 9700352 | tf_op jit(solution)/shard_map/dot_general | solution.py:105
  101.6 0.2 pad_convert_fusion
  101.7 6.0 %fusion.24 = f32[1536,256]{1,0:T(8,128)S(1)} fusion(f32[1566,256]{1,0:T(8,128)S(1)} %pad_convert_fusion, f32[256]{0:T(256)S(1)} %bitcast.62, f32[256]{0:T(256)S(1)} %bitcast.64, f32[256]{0:T(256)S(1)} %bitcast.65, f32[256]{0:T(256)S(1)} %bitcast.66, f32[256]{0:T(256)S(1)} %bitcast.67, f32[256]{0:T(256)S(1)} %bitcast.68, f32[256]{0:T(256)S(1)} %bitcast.69, ...), kind=kLoop, calls=%fused_computation.35 | loop fusion | flops 23986176 | bytes 50363392 | tf_op jit(solution)/shard_map/add | solution.py:56
  107.8 1.8 fusion.60
  109.6 0.9 fusion.54
  110.5 1.6 reshape.84
  112.1 0.4 reshape.85
  112.5 0.9 broadcast_in_dim.7
  113.4 4.3 %all-to-all-start.1 = ((f32[8,1,12288]{2,1,0:T(1,128)}), f32[8,1,12288]{2,1,0:T(1,128)S(1)}, u32[]{:S(2)}, u32[]{:S(2)}) async-start(f32[8,1,12288]{2,1,0:T(1,128)} %broadcast_in_dim.7), calls=%async_computation.1 | async-start | bytes 786432 | tf_op jit(solution)/shard_map/all_to_all | solution.py:28
  117.8 7.7 %all-to-all-done.1 = f32[8,1,12288]{2,1,0:T(1,128)S(1)} async-done(((f32[8,1,12288]{2,1,0:T(1,128)}), f32[8,1,12288]{2,1,0:T(1,128)S(1)}, u32[]{:S(2)}, u32[]{:S(2)}) %all-to-all-start.1) | async-done | bytes 393248 | tf_op jit(solution)/shard_map/all_to_all | solution.py:28
  125.5 0.3 reduce_sum.28
  125.8 0.8 div.26
  126.6 2.0 fusion.59
  128.6 0.8 div.28
  129.4 2.7 multiply_convert_fusion.2
  132.2 7.6 %convolution_multiply_fusion = f32[1536,2048]{1,0:T(8,128)} fusion(bf16[1536,256]{1,0:T(8,128)(2,1)S(1)} %multiply_convert_fusion.2, f32[2048]{0:T(1024)S(1)} %bitcast.48, bf16[2048,768]{0,1:T(8,128)(2,1)} %all-gather.3.cloned.1.call-done), kind=kOutput, calls=%fused_computation.1 | convolution fusion | flops 1613758464 | bytes 14426112 | tf_op jit(solution)/shard_map/dot_general | solution.py:120
  139.7 0.0 reduce-scatter.3.cloned.1.call-update
  139.7 0.0 all-gather.5.cloned.1.call-start
  139.8 1.0 copy-done.1
  140.7 0.2 copy.34
  141.0 0.8 pad_maximum_fusion
  141.8 71.1 %reduce-scatter.3.cloned.1.call-done = f32[192,2048]{1,0:T(8,128)} async-done(((f32[1536,2048]{1,0:T(8,128)}), f32[192,2048]{1,0:T(8,128)}) %reduce-scatter.3.cloned.1.call-update) | async-done | bytes 1572880 | tf_op jit(solution)/shard_map/reduce_scatter | solution.py:119
  212.9 1.7 fusion.20
  214.6 0.3 fusion.22
  214.9 3.5 broadcast_in_dim.8
  218.4 6.0 %all-to-all-start.2 = ((bf16[8,192,2048]{2,1,0:T(8,128)(2,1)}), bf16[8,192,2048]{2,1,0:T(8,128)(2,1)}, u32[]{:S(2)}, u32[]{:S(2)}) async-start(bf16[8,192,2048]{2,1,0:T(8,128)(2,1)} %broadcast_in_dim.8), calls=%async_computation.3 | async-start | bytes 12582912 | tf_op jit(solution)/shard_map/all_to_all | solution.py:28
  224.3 66.9 %all-gather.5.cloned.1.call-done = bf16[2048,2048]{0,1:T(8,128)(2,1)} async-done(((bf16[128,2048]{0,1:T(8,128)(2,1)}), bf16[2048,2048]{0,1:T(8,128)(2,1)}) %all-gather.5.cloned.1.call-update) | async-done | bytes 8388624 | tf_op jit(solution)/shard_map/all_gather | solution.py:12
  291.2 4.4 %all-to-all-done.2 = bf16[8,192,2048]{2,1,0:T(8,128)(2,1)} async-done(((bf16[8,192,2048]{2,1,0:T(8,128)(2,1)}), bf16[8,192,2048]{2,1,0:T(8,128)(2,1)}, u32[]{:S(2)}, u32[]{:S(2)}) %all-to-all-start.2) | async-done | bytes 6291488 | tf_op jit(solution)/shard_map/all_to_all | solution.py:28
  295.6 19.4 %multiply_convert_fusion = bf16[1536,2048]{1,0:T(8,128)(2,1)} fusion(f32[2048]{0:T(1024)S(1)} %bitcast.49, bf16[2048,2048]{0,1:T(8,128)(2,1)} %all-gather.5.cloned.1.call-done, bf16[1536,2048]{1,0:T(8,128)(2,1)} %bitcast.36, f32[1024]{0:T(1024)S(1)} %copy-done.7), kind=kOutput, calls=%fused_computation | convolution fusion | flops 12897484800 | bytes 20983808 | tf_op jit(solution)/shard_map/dot_general | solution.py:134
  315.1 41.8 %reduce-scatter.5.cloned.1.call-done = bf16[192,2048]{1,0:T(8,128)(2,1)} async-done(((bf16[1536,2048]{1,0:T(8,128)(2,1)}), bf16[192,2048]{1,0:T(8,128)(2,1)}) %reduce-scatter.5.cloned.1.call-update) | async-done | bytes 786448 | tf_op jit(solution)/shard_map/reduce_scatter | solution.py:133
  356.9 2.3 fusion.23
  (29 shorter events, 0.2 us)
Async XLA Ops:
  6.5 3.8 %copy-start = (bf16[192,2048]{1,0:T(8,128)(2,1)S(1)}, bf16[192,2048]{1,0:T(8,128)(2,1)}, u32[]{:S(2)}) copy-start(bf16[192,2048]{1,0:T(8,128)(2,1)} %param.15) | copy-start | bytes 2359300
  6.5 4.0 %copy-start.3 = (f32[2048]{0:T(1024)S(1)}, f32[2048]{0:T(1024)}, u32[]{:S(2)}) copy-start(f32[2048]{0:T(1024)} %param.16) | copy-start | bytes 24580
  6.5 85.2 %all-gather.3.cloned.1.call-start = ((), (), s32[]{:S(2)}) async-start(), calls=%async_computation.5 | async-start | bytes 3342336 | tf_op jit(solution)/shard_map/all_gather | solution.py:12
  14.3 8.4 %copy-start.5 = (f32[128]{0:T(128)S(1)}, f32[128]{0:T(128)}, u32[]{:S(2)}) copy-start(f32[128]{0:T(128)} %param.29) | copy-start | bytes 1540
  14.3 8.4 %copy-start.6 = (f32[128]{0:T(128)S(1)}, f32[128]{0:T(128)}, u32[]{:S(2)}) copy-start(f32[128]{0:T(128)} %param.24) | copy-start | bytes 1540
  14.3 77.4 %all-to-all-start = ((bf16[8,192,2048]{2,1,0:T(8,128)(2,1)}), bf16[8,192,2048]{2,1,0:T(8,128)(2,1)}, u32[]{:S(2)}, u32[]{:S(2)}) async-start(bf16[8,192,2048]{2,1,0:T(8,128)(2,1)} %broadcast_in_dim.6), calls=%async_computation | async-start | bytes 12582912 | tf_op jit(solution)/shard_map/all_to_all | solution.py:28
  113.4 12.0 %all-to-all-start.1 = ((f32[8,1,12288]{2,1,0:T(1,128)}), f32[8,1,12288]{2,1,0:T(1,128)S(1)}, u32[]{:S(2)}, u32[]{:S(2)}) async-start(f32[8,1,12288]{2,1,0:T(1,128)} %broadcast_in_dim.7), calls=%async_computation.1 | async-start | bytes 786432 | tf_op jit(solution)/shard_map/all_to_all | solution.py:28
  117.8 95.2 %reduce-scatter.3.cloned.1.call-start = ((), (), s32[]{:S(2)}) async-start(), calls=%async_computation.6 | async-start | bytes 14155776 | tf_op jit(solution)/shard_map/reduce_scatter | solution.py:119
  139.7 1.0 copy-start.1
  139.7 1.2 copy-start.2
  139.7 151.5 %all-gather.5.cloned.1.call-start = ((), (), s32[]{:S(2)}) async-start(), calls=%async_computation.7 | async-start | bytes 8912896 | tf_op jit(solution)/shard_map/all_gather | solution.py:12
  141.8 72.8 %copy-start.4 = (f32[2048]{0:T(1024)S(1)}, f32[2048]{0:T(1024)}, u32[]{:S(2)}) copy-start(f32[2048]{0:T(1024)} %param.25) | copy-start | bytes 24580
  218.4 77.2 %copy-start.7 = (f32[1024]{0:T(1024)S(1)}, f32[1024]{0:T(1024)}, u32[]{:S(2)}) copy-start(f32[1024]{0:T(1024)} %param.27) | copy-start | bytes 12292
  218.4 77.2 %all-to-all-start.2 = ((bf16[8,192,2048]{2,1,0:T(8,128)(2,1)}), bf16[8,192,2048]{2,1,0:T(8,128)(2,1)}, u32[]{:S(2)}, u32[]{:S(2)}) async-start(bf16[8,192,2048]{2,1,0:T(8,128)(2,1)} %broadcast_in_dim.8), calls=%async_computation.3 | async-start | bytes 12582912 | tf_op jit(solution)/shard_map/all_to_all | solution.py:28
  224.3 132.6 %reduce-scatter.5.cloned.1.call-start = ((), (), s32[]{:S(2)}) async-start(), calls=%async_computation.8 | async-start | bytes 7077888 | tf_op jit(solution)/shard_map/reduce_scatter | solution.py:133
Sparse Core Ops, SparseCore 0:
  10.4 53.8 all-gather.2
  139.9 73.0 reduce-scatter.2
  215.0 76.1 all-gather.4
  315.2 41.6 reduce-scatter.4
where the time goes:
time: 367 us; the launch traced here: 366 us
  waiting for transfers between devices  237 us (65%)
  matrix products  44.3 us (12%)
  blocking collectives  21.5 us (6%)
  local copies, waits for them, and re-layouts  19.2 us (5%)
  starting transfers between devices  16.5 us (4%)
  other arithmetic  13.8 us (4%)
  between operations  13.3 us (4%)
    reduce_scatter x1, waiting for transfers between devices, shards(): lax.psum_scatter(jnp.dot(act, point_rows, preferred_element_type=jnp.floa...  71.1 us
    all_gather x2, waiting for transfers between devices, gather_turned(): result, at, done = (lax.all_gather(both, axis, axis=0, tiled=True), 0, [])  66.9 us
    all_to_all x3, waiting for transfers between devices, from_everyone(): return lax.all_to_all(copies, axis, split_axis=0, concat_axis=0, tiled=True)  57.3 us
    reduce_scatter x1, waiting for transfers between devices, shards(): lax.psum_scatter((jnp.dot(hidden, down_part, preferred_element_type=jnp.f...  41.8 us
    all_gather x1, blocking collectives, gather_turned(): result, at, done = (lax.all_gather(both, axis, axis=0, tiled=True), 0, [])  21.5 us
    dot_general x1, matrix products, shards(): jnp.dot(hidden, down_part, preferred_element_type=jnp.float32) * down_full  19.4 us
    all_to_all x3, starting transfers between devices, from_everyone(): return lax.all_to_all(copies, axis, split_axis=0, concat_axis=0, tiled=True)  16.4 us
    broadcast_in_dim x3, local copies, waits for them, and re-layouts, from_everyone(): copies = jnp.broadcast_to(x, (lax.axis_size(axis), *x.shape))  7.88 us
  transfers between devices with their start and end apart: 7, of which 6 were waited for; matrix products, arithmetic and copies ran while one was open for 4% of the time, Pallas kernels for 0%

commit v1 on v0

--- a/solution.py
+++ b/solution.py
@@ -9,7 +9,13 @@
 def gather_turned(arrays, axis, dims):
     turned = [jnp.moveaxis(a, dim, 0) for a, dim in zip(arrays, dims)]
     both = jnp.concatenate([t.reshape(len(t), -1) for t in turned], axis=1)
-    result, at, done = (lax.all_gather(both, axis, axis=0, tiled=True), 0, [])
+    result, at, done = (
+        jnp.concatenate(
+            lax.all_to_all(jnp.stack([both] * lax.axis_size(axis)), axis, 0, 0), axis=0
+        ),
+        0,
+        [],
+    )
     for t, dim in zip(turned, dims):
         slab = result[:, at : at + t[0].size].reshape(-1, *t.shape[1:])
         done.append(jnp.moveaxis(slab, 0, dim))

time: 367 us -> 483 us (1.32)
  blocking collectives: 21.5 us -> 76.8 us
  waiting for transfers between devices: 237 us -> 282 us
  starting transfers between devices: 16.5 us -> 31 us
  local copies, waits for them, and re-layouts: 19.2 us -> 25.1 us
    all_to_all x0 -> x3, waiting for transfers between devices: none -> 107 us  [gather_turned(): lax.all_to_all(jnp.stack([both] * lax.axis_size(axis)), axis, 0, 0)]
    all_to_all x0 -> x1, blocking collectives: none -> 76.8 us  [from_everyone(): return lax.all_to_all(copies, axis, split_axis=0, concat_axis=0, tiled=True)]
    all_gather x2 -> x0, waiting for transfers between devices: 66.9 us -> none  [gather_turned(): result, at, done = (lax.all_gather(both, axis, axis=0, tiled=True), 0, [])]
    all_gather x1 -> x0, blocking collectives: 21.5 us -> none  [gather_turned(): result, at, done = (lax.all_gather(both, axis, axis=0, tiled=True), 0, [])]
    all_to_all x0 -> x3, starting transfers between devices: none -> 19.8 us  [gather_turned(): lax.all_to_all(jnp.stack([both] * lax.axis_size(axis)), axis, 0, 0)]
    all_to_all x3 -> x2, waiting for transfers between devices: 57.3 us -> 74.3 us  [from_everyone(): return lax.all_to_all(copies, axis, split_axis=0, concat_axis=0, tiled=True)]
    reduce_scatter x1, waiting for transfers between devices: 71.1 us -> 59.3 us  [shards(): lax.psum_scatter(jnp.dot(act, point_rows, preferred_element_type=jnp.floa...]
    another operation x0 -> x3, local copies, waits for them, and re-layouts: none -> 6.92 us  [gather_turned(): jnp.stack([both] * lax.axis_size(axis))]
  transfers between devices with their start and end apart: 7 -> 7, of which waited for: 6 -> 6; matrix products, arithmetic and copies ran while one was open for 4% -> 7% of each run, Pallas kernels for 0% -> 0%
where the time goes in v1:
time: 483 us; the launch traced here: 482 us
  waiting for transfers between devices  282 us (58%)
  blocking collectives  76.8 us (16%)
  matrix products  41.6 us (9%)
  starting transfers between devices  31 us (6%)
  local copies, waits for them, and re-layouts  25.1 us (5%)
  between operations  13.7 us (3%)
  other arithmetic  12.3 us (3%)
    all_to_all x3, waiting for transfers between devices, gather_turned(): lax.all_to_all(jnp.stack([both] * lax.axis_size(axis)), axis, 0, 0)  107 us
    all_to_all x1, blocking collectives, from_everyone(): return lax.all_to_all(copies, axis, split_axis=0, concat_axis=0, tiled=True)  76.8 us
    all_to_all x2, waiting for transfers between devices, from_everyone(): return lax.all_to_all(copies, axis, split_axis=0, concat_axis=0, tiled=True)  74.3 us
    reduce_scatter x1, waiting for transfers between devices, shards(): lax.psum_scatter(jnp.dot(act, point_rows, preferred_element_type=jnp.floa...  59.3 us
    reduce_scatter x1, waiting for transfers between devices, shards(): lax.psum_scatter((jnp.dot(hidden, down_part, preferred_element_type=jnp.f...  41.1 us
    all_to_all x3, starting transfers between devices, gather_turned(): lax.all_to_all(jnp.stack([both] * lax.axis_size(axis)), axis, 0, 0)  19.8 us
    dot_general x1, matrix products, shards(): jnp.dot(hidden, down_part, preferred_element_type=jnp.float32) * down_full  19.4 us
    all_to_all x2, starting transfers between devices, from_everyone(): return lax.all_to_all(copies, axis, split_axis=0, concat_axis=0, tiled=True)  11.1 us
  transfers between devices with their start and end apart: 7, of which 6 were waited for; matrix products, arithmetic and copies ran while one was open for 7% of the time, Pallas kernels for 0%

profile of v1, /device:TPU:1, one launch (start us, length us, event | category | flops | bytes accessed | tf_op | source)
XLA Modules:
  0.0 481.9 jit_solution(14014560609665285897)
XLA Ops:
  6.5 0.9 convert_bitcast_fusion.1
  7.4 1.0 copy.44
  8.5 1.0 copy.43
  9.7 2.0 stack.6
  11.6 8.8 %all-to-all-start.1 = ((bf16[16,128,768]{2,1,0:T(8,128)(2,1)}), bf16[16,128,768]{2,1,0:T(8,128)(2,1)}, u32[]{:S(2)}, u32[]{:S(2)}) async-start(bf16[16,128,768]{2,1,0:T(8,128)(2,1)} %stack.6), calls=%async_computation.1 | async-start | bytes 6291456 | tf_op jit(solution)/shard_map/all_to_all | solution.py:14
  20.4 0.2 fusion.16
  20.7 0.3 fusion.18
  20.9 46.4 %all-to-all-done.1 = bf16[16,128,768]{2,1,0:T(8,128)(2,1)} async-done(((bf16[16,128,768]{2,1,0:T(8,128)(2,1)}), bf16[16,128,768]{2,1,0:T(8,128)(2,1)}, u32[]{:S(2)}, u32[]{:S(2)}) %all-to-all-start.1) | async-done | bytes 3145760 | tf_op jit(solution)/shard_map/all_to_all | solution.py:14
  67.3 3.4 broadcast_in_dim.6
  70.7 6.5 %all-to-all-start = ((bf16[8,192,2048]{2,1,0:T(8,128)(2,1)}), bf16[8,192,2048]{2,1,0:T(8,128)(2,1)}, u32[]{:S(2)}, u32[]{:S(2)}) async-start(bf16[8,192,2048]{2,1,0:T(8,128)(2,1)} %broadcast_in_dim.6), calls=%async_computation | async-start | bytes 12582912 | tf_op jit(solution)/shard_map/all_to_all | solution.py:34
  77.3 0.8 dynamic_slice.14
  78.0 0.8 dynamic_slice.13
  78.8 0.8 dynamic_slice.15
  79.6 1.2 fusion.68
  80.8 1.2 constant_dynamic-slice_fusion
  82.0 66.6 %all-to-all-done = bf16[8,192,2048]{2,1,0:T(8,128)(2,1)} async-done(((bf16[8,192,2048]{2,1,0:T(8,128)(2,1)}), bf16[8,192,2048]{2,1,0:T(8,128)(2,1)}, u32[]{:S(2)}, u32[]{:S(2)}) %all-to-all-start) | async-done | bytes 6291488 | tf_op jit(solution)/shard_map/all_to_all | solution.py:34
  148.6 0.6 stack.7
  149.2 4.1 all-to-all-start.3
  153.2 4.9 %fusion.14 = f32[1536,256]{1,0:T(8,128)S(1)} fusion(bf16[1536,2048]{1,0:T(8,128)(2,1)} %bitcast.1, bf16[2048,768]{1,0:T(8,128)(2,1)} %bitcast.3, f32[256]{0:T(256)S(1)} %dynamic_slice.14), kind=kOutput, calls=%fused_computation.18 | convolution fusion | flops 1612185600 | bytes 8913920 | tf_op jit(solution)/shard_map/dot_general | solution.py:112
  158.2 4.8 %fusion.15 = bf16[1536,256]{1,0:T(8,128)(2,1)S(1)} fusion(f32[1536,256]{1,0:T(8,128)S(1)} %fusion.14, bf16[1536,2048]{1,0:T(8,128)(2,1)} %bitcast.1, bf16[2048,768]{1,0:T(8,128)(2,1)} %bitcast.3, f32[256]{0:T(256)S(1)} %dynamic_slice.13), kind=kOutput, calls=%fused_computation.19 | convolution fusion | flops 1611792384 | bytes 9700352 | tf_op jit(solution)/shard_map/dot_general | solution.py:111
  163.2 6.0 %fusion.24 = f32[1536,256]{1,0:T(8,128)S(1)} fusion(f32[1566,256]{1,0:T(8,128)S(1)} %pad_convert_fusion, f32[256]{0:T(256)S(1)} %bitcast.67, f32[256]{0:T(256)S(1)} %bitcast.69, f32[256]{0:T(256)S(1)} %bitcast.70, f32[256]{0:T(256)S(1)} %bitcast.71, f32[256]{0:T(256)S(1)} %bitcast.72, f32[256]{0:T(256)S(1)} %bitcast.73, f32[256]{0:T(256)S(1)} %bitcast.74, ...), kind=kLoop, calls=%fused_computation.35 | loop fusion | flops 23986176 | bytes 50363392 | tf_op jit(solution)/shard_map/add | solution.py:62
  169.2 1.8 fusion.54
  171.0 0.9 fusion.60
  171.9 1.6 reshape.101
  173.5 0.4 reshape.100
  173.9 0.9 broadcast_in_dim.7
  174.9 4.6 all-to-all-start.2
  179.5 7.7 %all-to-all-done.2 = f32[8,1,12288]{2,1,0:T(1,128)S(1)} async-done(((f32[8,1,12288]{2,1,0:T(1,128)}), f32[8,1,12288]{2,1,0:T(1,128)S(1)}, u32[]{:S(2)}, u32[]{:S(2)}) %all-to-all-start.2) | async-done | bytes 393248 | tf_op jit(solution)/shard_map/all_to_all | solution.py:34
  187.2 0.3 reduce_sum.28
  187.5 1.7 div.28
  189.2 0.8 div.26
  190.0 0.9 fusion.59
  190.9 0.3 copy-done.1
  191.1 1.3 multiply_convert_fusion.2
  192.5 7.6 %convolution_multiply_fusion = f32[1536,2048]{1,0:T(8,128)} fusion(bf16[1536,256]{1,0:T(8,128)(2,1)S(1)} %multiply_convert_fusion.2, f32[2048]{0:T(1024)S(1)} %bitcast.52, bf16[2048,768]{1,0:T(8,128)(2,1)} %bitcast.3), kind=kOutput, calls=%fused_computation.1 | convolution fusion | flops 1613758464 | bytes 14426112 | tf_op jit(solution)/shard_map/dot_general | solution.py:126
  200.1 1.0 copy-done.2
  201.4 0.2 copy.50
  201.6 4.4 stack.8
  205.9 7.0 %all-to-all-start.5 = ((bf16[16,128,2048]{2,1,0:T(8,128)(2,1)}), bf16[16,128,2048]{2,1,0:T(8,128)(2,1)}, u32[]{:S(2)}, u32[]{:S(2)}) async-start(bf16[16,128,2048]{2,1,0:T(8,128)(2,1)} %stack.8), calls=%async_computation.6 | async-start | bytes 16777216 | tf_op jit(solution)/shard_map/all_to_all | solution.py:14
  213.0 59.3 %reduce-scatter.3.cloned.1.call-done = f32[192,2048]{1,0:T(8,128)} async-done(((f32[1536,2048]{1,0:T(8,128)}), f32[192,2048]{1,0:T(8,128)}) %reduce-scatter.3.cloned.1.call-update) | async-done | bytes 1572880 | tf_op jit(solution)/shard_map/reduce_scatter | solution.py:125
  272.3 1.7 fusion.20
  274.0 0.3 fusion.22
  274.3 60.4 %all-to-all-done.5 = bf16[16,128,2048]{2,1,0:T(8,128)(2,1)} async-done(((bf16[16,128,2048]{2,1,0:T(8,128)(2,1)}), bf16[16,128,2048]{2,1,0:T(8,128)(2,1)}, u32[]{:S(2)}, u32[]{:S(2)}) %all-to-all-start.5) | async-done | bytes 8388640 | tf_op jit(solution)/shard_map/all_to_all | solution.py:14
  334.7 0.8 broadcast_in_dim.8
  335.5 76.8 %all_to_all.31 = bf16[8,192,2048]{2,1,0:T(8,128)(2,1)} all-to-all(bf16[8,192,2048]{2,1,0:T(8,128)(2,1)S(1)} %broadcast_in_dim.8), channel_id=1, replica_groups=mesh['fs'=16,'tp'=8] {'tp'}, dimensions={0} | all-to-all | bytes 12582912 | tf_op jit(solution)/shard_map/all_to_all | solution.py:34
  412.3 19.4 %multiply_convert_fusion = bf16[1536,2048]{1,0:T(8,128)(2,1)} fusion(f32[2048]{0:T(1024)S(1)} %bitcast.54, bf16[2048,2048]{1,0:T(8,128)(2,1)} %bitcast.40, bf16[1536,2048]{1,0:T(8,128)(2,1)} %bitcast.51, f32[1024]{0:T(1024)S(1)} %copy-done.8), kind=kOutput, calls=%fused_computation | convolution fusion | flops 12897484800 | bytes 20983808 | tf_op jit(solution)/shard_map/dot_general | solution.py:140
  431.7 41.1 %reduce-scatter.5.cloned.1.call-done = bf16[192,2048]{1,0:T(8,128)(2,1)} async-done(((bf16[1536,2048]{1,0:T(8,128)(2,1)}), bf16[192,2048]{1,0:T(8,128)(2,1)}) %reduce-scatter.5.cloned.1.call-update) | async-done | bytes 786448 | tf_op jit(solution)/shard_map/reduce_scatter | solution.py:139
  472.8 2.3 fusion.23
  (34 shorter events, 0.7 us)
Async XLA Ops:
  11.6 8.8 %copy-start = (bf16[192,2048]{1,0:T(8,128)(2,1)S(1)}, bf16[192,2048]{1,0:T(8,128)(2,1)}, u32[]{:S(2)}) copy-start(bf16[192,2048]{1,0:T(8,128)(2,1)} %param.15) | copy-start | bytes 2359300
  11.6 9.0 %copy-start.4 = (f32[2048]{0:T(1024)S(1)}, f32[2048]{0:T(1024)}, u32[]{:S(2)}) copy-start(f32[2048]{0:T(1024)} %param.16) | copy-start | bytes 24580
  11.6 55.7 %all-to-all-start.1 = ((bf16[16,128,768]{2,1,0:T(8,128)(2,1)}), bf16[16,128,768]{2,1,0:T(8,128)(2,1)}, u32[]{:S(2)}, u32[]{:S(2)}) async-start(bf16[16,128,768]{2,1,0:T(8,128)(2,1)} %stack.6), calls=%async_computation.1 | async-start | bytes 6291456 | tf_op jit(solution)/shard_map/all_to_all | solution.py:14
  70.7 8.8 %copy-start.6 = (f32[128]{0:T(128)S(1)}, f32[128]{0:T(128)}, u32[]{:S(2)}) copy-start(f32[128]{0:T(128)} %param.29) | copy-start | bytes 1540
  70.7 8.8 %copy-start.7 = (f32[128]{0:T(128)S(1)}, f32[128]{0:T(128)}, u32[]{:S(2)}) copy-start(f32[128]{0:T(128)} %param.24) | copy-start | bytes 1540
  70.7 77.8 %all-to-all-start = ((bf16[8,192,2048]{2,1,0:T(8,128)(2,1)}), bf16[8,192,2048]{2,1,0:T(8,128)(2,1)}, u32[]{:S(2)}, u32[]{:S(2)}) async-start(bf16[8,192,2048]{2,1,0:T(8,128)(2,1)} %broadcast_in_dim.6), calls=%async_computation | async-start | bytes 12582912 | tf_op jit(solution)/shard_map/all_to_all | solution.py:34
  149.2 24.8 %all-to-all-start.3 = ((f32[16,128,2]{1,2,0:T(2,128)}), f32[16,128,2]{1,2,0:T(2,128)S(1)}, u32[]{:S(2)}, u32[]{:S(2)}) async-start(f32[16,128,2]{1,2,0:T(2,128)} %stack.7), calls=%async_computation.3 | async-start | bytes 32768 | tf_op jit(solution)/shard_map/all_to_all | solution.py:14
  174.9 12.3 %all-to-all-start.2 = ((f32[8,1,12288]{2,1,0:T(1,128)}), f32[8,1,12288]{2,1,0:T(1,128)S(1)}, u32[]{:S(2)}, u32[]{:S(2)}) async-start(f32[8,1,12288]{2,1,0:T(1,128)} %broadcast_in_dim.7), calls=%async_computation.2 | async-start | bytes 786432 | tf_op jit(solution)/shard_map/all_to_all | solution.py:34
  179.5 92.8 %reduce-scatter.3.cloned.1.call-start = ((), (), s32[]{:S(2)}) async-start(), calls=%async_computation.8 | async-start | bytes 14155776 | tf_op jit(solution)/shard_map/reduce_scatter | solution.py:125
  190.0 1.1 copy-start.1
  200.1 1.0 copy-start.2
  200.1 1.2 copy-start.3
  205.9 128.8 %all-to-all-start.5 = ((bf16[16,128,2048]{2,1,0:T(8,128)(2,1)}), bf16[16,128,2048]{2,1,0:T(8,128)(2,1)}, u32[]{:S(2)}, u32[]{:S(2)}) async-start(bf16[16,128,2048]{2,1,0:T(8,128)(2,1)} %stack.8), calls=%async_computation.6 | async-start | bytes 16777216 | tf_op jit(solution)/shard_map/all_to_all | solution.py:14
  212.9 61.1 %copy-start.5 = (f32[2048]{0:T(1024)S(1)}, f32[2048]{0:T(1024)}, u32[]{:S(2)}) copy-start(f32[2048]{0:T(1024)} %param.25) | copy-start | bytes 24580
  213.0 259.9 %reduce-scatter.5.cloned.1.call-start = ((), (), s32[]{:S(2)}) async-start(), calls=%async_computation.9 | async-start | bytes 7077888 | tf_op jit(solution)/shard_map/reduce_scatter | solution.py:139
  335.5 76.8 %copy-start.8 = (f32[1024]{0:T(1024)S(1)}, f32[1024]{0:T(1024)}, u32[]{:S(2)}) copy-start(f32[1024]{0:T(1024)} %param.27) | copy-start | bytes 12292
Sparse Core Ops, SparseCore 0:
  200.2 72.0 reduce-scatter.2
  431.8 40.9 reduce-scatter.4
